TPU v7x, 32 devices: a whole 2x2x4 slice. The times are simulated.
32 devices in a mesh: ep: 8 (over z, y), tp: 4 (over x, core).
Axes of the slice: x: 2, y: 2, z: 4, core: 2. Of those that a mesh axis runs over, the one named last changes fastest.
Arguments:
- tokens: bfloat16 [1024, 2048], P('ep', 'tp'), may hold values from -6 to 6
- norm_gain: bfloat16 [2048], P('tp'), may hold values from 0.099609375 to 1.8984375
- routes: int32 [1024, 2], P('ep'), may hold values from 0 to 7, as said below
- gate_weights: float32 [1024, 2], P('ep'), may hold values from 0.1 to 1
- w_gate: bfloat16 [8, 2048, 4096], P('ep', None, 'tp'), may hold values from -0.125 to 0.125
- w_up: bfloat16 [8, 2048, 4096], P('ep', None, 'tp'), may hold values from -0.125 to 0.125
- w_down: bfloat16 [8, 4096, 2048], P('ep', 'tp'), may hold values from -0.875 to 0.875
- out_gain: bfloat16 [2048], P('tp'), may hold values from 0.099609375 to 1.8984375
Outputs:
- mixed: bfloat16 [1024, 2048], P('ep', 'tp')
Inputs may be any that keep to these rules, and one draw needn't show every extreme that they name: `routes`: each row names 2 different experts of one group (their quotients by 8 agree). In each aligned block of 128 rows no expert is named by more than 64 rows, and in every block some expert is named by exactly 64 rows.
All inputs are finite; a program needn't handle non-finite values.
Results may differ from a plain program's by a relative error of at most 0.019.
Values may be sent and summed in bfloat16 or wider, within the bound.
A program may use at most 64 MiB of HBM per device.

v0:
```python
import jax
import jax.numpy as jnp
from jax import lax
from jax.sharding import PartitionSpec as P

epsilon = 1e-06


def shards(tokens, norm_gain, routes, gate_weights, w_gate, w_up, w_down, out_gain):
    tok_rows = tokens.shape[0]
    width_local = tokens.shape[1]
    full_width = width_local * lax.axis_size("tp")
    experts = lax.axis_size("ep")
    top_count = routes.shape[1]
    capacity = 2 * top_count * tok_rows // experts
    flat_ids = routes.reshape(-1)
    onehot = (flat_ids[:, None] == jnp.arange(experts, dtype=jnp.int32)[None, :]).astype(jnp.int32)
    before = jnp.cumsum(onehot, axis=0) - onehot
    slot_index = jnp.sum(before * onehot, axis=1)
    dest_index = flat_ids * capacity + slot_index
    dest_pairs = dest_index.reshape(tok_rows, top_count)
    places = jnp.arange(experts * capacity, dtype=jnp.int32)
    scatter_mat = jnp.any(dest_pairs[None, :, :] == places[:, None, None], axis=2).astype(
        jnp.bfloat16
    )
    gate_mat = w_gate[0]
    up_mat = w_up[0]
    x_float = tokens.astype(jnp.float32)
    row_sums = lax.psum(jnp.sum(x_float * x_float, axis=1), "tp")
    scale_in = lax.rsqrt(row_sums / full_width + epsilon)
    normed = (x_float * scale_in[:, None] * norm_gain.astype(jnp.float32)).astype(jnp.bfloat16)
    outgoing = jnp.dot(scatter_mat, normed, preferred_element_type=jnp.float32).astype(jnp.bfloat16)
    arrived = lax.all_to_all(outgoing, "ep", split_axis=0, concat_axis=0, tiled=True)
    portion = lax.all_gather(arrived, "tp", axis=1, tiled=True)
    gate_sum = jnp.dot(portion, gate_mat, preferred_element_type=jnp.float32)
    up_sum = jnp.dot(portion, up_mat, preferred_element_type=jnp.float32)
    hidden = (jax.nn.silu(gate_sum) * up_sum).astype(jnp.bfloat16)
    down_mat = w_down[0]
    summed = lax.psum_scatter(
        lax.dot_general(
            down_mat, hidden, (((0,), (1,)), ((), ())), preferred_element_type=jnp.float32
        ).astype(jnp.bfloat16),
        "tp",
        scatter_dimension=0,
        tiled=True,
    )
    came_back = lax.all_to_all(summed, "ep", split_axis=1, concat_axis=1, tiled=True)
    picked = (
        jnp.take(came_back, dest_index, axis=1)
        .astype(jnp.float32)
        .reshape(width_local, tok_rows, top_count)
    )
    combined = jnp.sum(picked * gate_weights[None, :, :], axis=2).T
    out_sums = lax.psum(jnp.sum(combined * combined, axis=1), "tp")
    scale_out = lax.rsqrt(out_sums / full_width + epsilon)
    return (combined * scale_out[:, None] * out_gain.astype(jnp.float32)).astype(jnp.bfloat16)


def solution(mesh):
    placed = (
        P("ep", "tp"),
        P("tp"),
        P("ep", None),
        P("ep", None),
        P("ep", None, "tp"),
        P("ep", None, "tp"),
        P("ep", "tp", None),
        P("tp"),
    )
    return jax.shard_map(
        shards, mesh=mesh, in_specs=placed, out_specs=P("ep", "tp"), check_vma=False
    )
```

profile of v0, /device:TPU:0, one launch (start us, length us, event | category | flops | bytes accessed | tf_op | source)
XLA Modules:
  0.0 145.3 jit_solution(15379768702945613426)
XLA Ops:
  6.5 0.8 copy.21
  7.3 0.1 eq.39
  7.5 0.1 reshape.77
  7.6 0.6 reduce-window.6
  8.2 0.2 slice_reduce_fusion
  8.5 0.1 fusion.25
  8.6 0.1 reduce_sum.41
  8.7 0.1 copy.23
  8.8 0.7 compare_and_fusion
  9.5 0.1 fusion.16
  9.5 0.7 convert_element_type.45
  10.2 1.0 fusion.17
  11.2 8.4 %psum.14 = f32[128]{0:T(128)S(1)} all-reduce(f32[128]{0:T(128)S(1)} %fusion.17), channel_id=1, replica_groups=mesh['ep'=8,'tp'=4] {'tp'}, use_global_device_ids=true, to_apply=%region_5.6 | all-reduce | flops 128 | bytes 1024 | tf_op jit(solution)/shard_map/psum | solution.py:29
  19.6 1.3 convolution_convert_fusion
  20.9 19.0 %all_to_all.24 = bf16[8,64,512]{2,1,0:T(8,128)(2,1)} all-to-all(bf16[8,64,512]{2,1,0:T(8,128)(2,1)S(1)} %bitcast.43), channel_id=1, replica_groups=mesh['ep'=8,'tp'=4] {'ep'}, dimensions={0} | all-to-all | bytes 1048576 | tf_op jit(solution)/shard_map/all_to_all | solution.py:33
  39.9 0.0 reduce-scatter.2.cloned.1.call-start
  40.0 21.8 %all-gather.2.cloned.1.call-done = bf16[512,2048]{1,0:T(8,128)(2,1)} async-done(((bf16[512,512]{1,0:T(8,128)(2,1)}), bf16[512,2048]{1,0:T(8,128)(2,1)}) %all-gather.2.cloned.1.call-update) | async-done | bytes 2097168 | tf_op jit(solution)/shard_map/all_gather | solution.py:34
  61.7 6.6 %fusion.4 = f32[512,1024]{1,0:T(8,128)} fusion(bf16[512,2048]{1,0:T(8,128)(2,1)} %all-gather.2.cloned.1.call-done, bf16[1,2048,1024]{2,1,0:T(8,128)(2,1)} %param.12), kind=kOutput, calls=%fused_computation.5 | convolution fusion | flops 2147483648 | bytes 8388608 | tf_op jit(solution)/shard_map/dot_general | solution.py:35
  68.3 10.0 %fusion.9 = bf16[2048,512]{0,1:T(8,128)(2,1)} fusion(bf16[1,1024,2048]{2,1,0:T(8,128)(2,1)} %param.14, f32[512,1024]{1,0:T(8,128)} %fusion.4, bf16[512,2048]{1,0:T(8,128)(2,1)S(1)} %copy-done.3, bf16[1,2048,1024]{2,1,0:T(8,128)(2,1)} %param.13), kind=kOutput, calls=%fused_computation.8 | convolution fusion | flops 4299161600 | bytes 14680064 | tf_op jit(solution)/shard_map/dot_general | solution.py:40
  78.4 31.3 %reduce-scatter.2.cloned.1.call-done = bf16[512,512]{0,1:T(8,128)(2,1)} async-done(((bf16[2048,512]{0,1:T(8,128)(2,1)}), bf16[512,512]{0,1:T(8,128)(2,1)}) %reduce-scatter.2.cloned.1.call-update) | async-done | bytes 524304 | tf_op jit(solution)/shard_map/reduce_scatter | solution.py:39
  109.7 5.5 %all-to-all-start.1 = ((bf16[512,8,64]{0,2,1:T(8,128)(2,1)}), bf16[512,8,64]{0,2,1:T(8,128)(2,1)S(1)}, u32[]{:S(2)}, u32[]{:S(2)}) async-start(bf16[512,8,64]{0,2,1:T(8,128)(2,1)} %bitcast.45), calls=%async_computation.2 | async-start | bytes 1048576 | tf_op jit(solution)/shard_map/all_to_all | solution.py:47
  115.2 0.1 copy.25
  115.4 0.1 mul.90
  115.5 0.1 copy.24
  115.6 0.1 copy.26
  115.8 13.7 %all-to-all-done.1 = bf16[512,8,64]{0,2,1:T(8,128)(2,1)S(1)} async-done(((bf16[512,8,64]{0,2,1:T(8,128)(2,1)}), bf16[512,8,64]{0,2,1:T(8,128)(2,1)S(1)}, u32[]{:S(2)}, u32[]{:S(2)}) %all-to-all-start.1) | async-done | bytes 524320 | tf_op jit(solution)/shard_map/all_to_all | solution.py:47
  129.5 1.2 gather_fusion
  130.7 0.1 gather.7
  130.8 0.8 multiply_reduce_fusion
  131.7 0.1 multiply_reduce_fusion.1
  131.8 6.0 %psum.15 = f32[128]{0:T(128)S(1)} all-reduce(f32[128]{0:T(128)S(1)} %multiply_reduce_fusion.1), channel_id=1, replica_groups=mesh['ep'=8,'tp'=4] {'tp'}, use_global_device_ids=true, to_apply=%region_9.10 | all-reduce | flops 128 | bytes 1024 | tf_op jit(solution)/shard_map/psum | solution.py:54
  137.7 0.8 fusion.20
  (20 shorter events, 0.1 us)
Async XLA Ops:
  6.5 55.2 %all-gather.2.cloned.1.call-start = ((), (), s32[]{:S(2)}) async-start(), calls=%async_computation.3 | async-start | bytes 2621440 | tf_op jit(solution)/shard_map/all_gather | solution.py:34
  39.9 69.8 %reduce-scatter.2.cloned.1.call-start = ((), (), s32[]{:S(2)}) async-start(), calls=%async_computation.4 | async-start | bytes 2621440 | tf_op jit(solution)/shard_map/reduce_scatter | solution.py:39
  61.7 6.6 %copy-start.3 = (bf16[512,2048]{1,0:T(8,128)(2,1)S(1)}, bf16[512,2048]{1,0:T(8,128)(2,1)}, u32[]{:S(2)}) copy-start(bf16[512,2048]{1,0:T(8,128)(2,1)} %all-gather.2.cloned.1.call-done) | copy-start | bytes 6291460
  78.3 36.9 %copy-start = (s32[128,2]{0,1:T(2,128)S(1)}, s32[128,2]{0,1:T(2,128)}, u32[]{:S(2)}) copy-start(s32[128,2]{0,1:T(2,128)} %param.10) | copy-start | bytes 3076
  78.3 37.3 %copy-start.1 = (f32[128,2]{0,1:T(2,128)S(1)}, f32[128,2]{0,1:T(2,128)}, u32[]{:S(2)}) copy-start(f32[128,2]{0,1:T(2,128)} %param.11) | copy-start | bytes 3076
  78.3 37.4 %copy-start.2 = (bf16[512]{0:T(512)(128)(2,1)S(1)}, bf16[512]{0:T(512)(128)(2,1)}, u32[]{:S(2)}) copy-start(bf16[512]{0:T(512)(128)(2,1)} %param.15) | copy-start | bytes 3076
  109.7 19.8 %all-to-all-start.1 = ((bf16[512,8,64]{0,2,1:T(8,128)(2,1)}), bf16[512,8,64]{0,2,1:T(8,128)(2,1)S(1)}, u32[]{:S(2)}, u32[]{:S(2)}) async-start(bf16[512,8,64]{0,2,1:T(8,128)(2,1)} %bitcast.45), calls=%async_computation.2 | async-start | bytes 1048576 | tf_op jit(solution)/shard_map/all_to_all | solution.py:47
Sparse Core Ops, SparseCore 0:
  40.1 21.6 all-gather.1
  78.5 31.1 reduce-scatter.1
where the time goes:
time: 146 us; the launch traced here: 145 us
  waiting for transfers between devices  66.9 us (46%)
  blocking collectives  33.3 us (23%)
  matrix products  17.9 us (12%)
  between operations  13.5 us (9%)
  starting transfers between devices  5.56 us (4%)
  other arithmetic  4.93 us (3%)
  local copies, waits for them, and re-layouts  3.25 us (2%)
    reduce_scatter x1, waiting for transfers between devices, shards(): lax.psum_scatter(lax.dot_general(down_mat, hidden, (((0,), (1,)), ((), ()...  31.3 us
    all_gather x1, waiting for transfers between devices, shards(): portion = lax.all_gather(arrived, 'tp', axis=1, tiled=True)  21.8 us
    all_to_all x1, blocking collectives, shards(): lax.all_to_all(outgoing, 'ep', split_axis=0, concat_axis=0, tiled=True)  19 us
    all_to_all x1, waiting for transfers between devices, shards(): lax.all_to_all(summed, 'ep', split_axis=1, concat_axis=1, tiled=True)  13.7 us
    dot_general x1, matrix products, shards(): lax.dot_general(down_mat, hidden, (((0,), (1,)), ((), ())), preferred_ele...  10 us
    psum x1, blocking collectives, shards(): row_sums = lax.psum(jnp.sum(x_float * x_float, axis=1), 'tp')  8.37 us
    dot_general x1, matrix products, shards(): gate_sum = jnp.dot(portion, gate_mat, preferred_element_type=jnp.float32)  6.59 us
    psum x1, blocking collectives, shards(): out_sums = lax.psum(jnp.sum(combined * combined, axis=1), 'tp')  5.95 us
  transfers between devices with their start and end apart: 3, of which 3 were waited for; matrix products, arithmetic and copies ran while one was open for 0% of the time, Pallas kernels for 0%

commit v1 on v0

--- a/solution.py
+++ b/solution.py
@@ -1,9 +1,17 @@
+import functools
 import jax
 import jax.numpy as jnp
 from jax import lax
 from jax.sharding import PartitionSpec as P
 
 epsilon = 1e-06
+
+
+def _guide_screen(inputs, lane_axis):
+    return jnp.sum(lax.all_gather(inputs, lane_axis), axis=0)
+
+
+assign_tokens_in = functools.partial(_guide_screen, lane_axis="tp")
 
 
 def shards(tokens, norm_gain, routes, gate_weights, w_gate, w_up, w_down, out_gain):
@@ -26,7 +34,7 @@
     gate_mat = w_gate[0]
     up_mat = w_up[0]
     x_float = tokens.astype(jnp.float32)
-    row_sums = lax.psum(jnp.sum(x_float * x_float, axis=1), "tp")
+    row_sums = assign_tokens_in(jnp.sum(x_float * x_float, axis=1))
     scale_in = lax.rsqrt(row_sums / full_width + epsilon)
     normed = (x_float * scale_in[:, None] * norm_gain.astype(jnp.float32)).astype(jnp.bfloat16)
     outgoing = jnp.dot(scatter_mat, normed, preferred_element_type=jnp.float32).astype(jnp.bfloat16)

time: 146 us -> 146 us (level)
    psum x1 -> x0, blocking collectives: 8.37 us -> none  [shards(): row_sums = lax.psum(jnp.sum(x_float * x_float, axis=1), 'tp')]
    all_gather x0 -> x1, blocking collectives: none -> 6.01 us  [_guide_screen(): return jnp.sum(lax.all_gather(inputs, lane_axis), axis=0)]
    all_to_all x1, blocking collectives: 19 us -> 21.3 us  [shards(): lax.all_to_all(outgoing, 'ep', split_axis=0, concat_axis=0, tiled=True)]
where the time goes in v1:
time: 146 us; the launch traced here: 145 us
  waiting for transfers between devices  66.8 us (46%)
  blocking collectives  33.2 us (23%)
  matrix products  17.9 us (12%)
  between operations  13.5 us (9%)
  starting transfers between devices  5.56 us (4%)
  other arithmetic  4.95 us (3%)
  local copies, waits for them, and re-layouts  3.25 us (2%)
    reduce_scatter x1, waiting for transfers between devices, shards(): lax.psum_scatter(lax.dot_general(down_mat, hidden, (((0,), (1,)), ((), ()...  31.3 us
    all_gather x1, waiting for transfers between devices, shards(): portion = lax.all_gather(arrived, 'tp', axis=1, tiled=True)  21.7 us
    all_to_all x1, blocking collectives, shards(): lax.all_to_all(outgoing, 'ep', split_axis=0, concat_axis=0, tiled=True)  21.3 us
    all_to_all x1, waiting for transfers between devices, shards(): lax.all_to_all(summed, 'ep', split_axis=1, concat_axis=1, tiled=True)  13.7 us
    dot_general x1, matrix products, shards(): lax.dot_general(down_mat, hidden, (((0,), (1,)), ((), ())), preferred_ele...  10 us
    dot_general x1, matrix products, shards(): gate_sum = jnp.dot(portion, gate_mat, preferred_element_type=jnp.float32)  6.59 us
    all_gather x1, blocking collectives, _guide_screen(): return jnp.sum(lax.all_gather(inputs, lane_axis), axis=0)  6.01 us
    psum x1, blocking collectives, shards(): out_sums = lax.psum(jnp.sum(combined * combined, axis=1), 'tp')  5.94 us
  transfers between devices with their start and end apart: 3, of which 3 were waited for; matrix products, arithmetic and copies ran while one was open for 0% of the time, Pallas kernels for 0%

profile of v1, /device:TPU:0, one launch (start us, length us, event | category | flops | bytes accessed | tf_op | source)
XLA Modules:
  0.0 145.2 jit_solution(2727997254043128989)
XLA Ops:
  6.5 0.8 copy.25
  7.3 0.1 eq.39
  7.5 0.1 reshape.81
  7.6 0.6 reduce-window.6
  8.2 0.2 slice_reduce_fusion
  8.5 0.1 fusion.25
  8.6 0.1 reduce_sum.50
  8.7 0.1 copy.27
  8.8 0.7 compare_and_fusion
  9.5 0.1 fusion.16
  9.5 1.0 fusion.17
  10.6 6.0 %all-gather.1 = f32[4,1,128]{2,1,0:T(1,128)S(1)} all-gather(f32[1,1,128]{2,1,0:T(1,128)S(1)} %bitcast.49), channel_id=2, replica_groups=mesh['ep'=8,'tp'=4] {'tp'}, dimensions={0}, use_global_device_ids=true | all-gather | bytes 2560 | tf_op jit(solution)/shard_map/all_gather | solution.py:11
  16.6 0.7 convert_element_type.45
  17.3 1.3 convolution_convert_fusion
  18.6 21.3 %all_to_all.24 = bf16[8,64,512]{2,1,0:T(8,128)(2,1)} all-to-all(bf16[8,64,512]{2,1,0:T(8,128)(2,1)S(1)} %bitcast.44), channel_id=1, replica_groups=mesh['ep'=8,'tp'=4] {'ep'}, dimensions={0} | all-to-all | bytes 1048576 | tf_op jit(solution)/shard_map/all_to_all | solution.py:41
  39.8 0.0 reduce-scatter.2.cloned.1.call-start
  39.9 21.7 %all-gather.4.cloned.1.call-done = bf16[512,2048]{1,0:T(8,128)(2,1)} async-done(((bf16[512,512]{1,0:T(8,128)(2,1)}), bf16[512,2048]{1,0:T(8,128)(2,1)}) %all-gather.4.cloned.1.call-update) | async-done | bytes 2097168 | tf_op jit(solution)/shard_map/all_gather | solution.py:42
  61.6 6.6 %fusion.4 = f32[512,1024]{1,0:T(8,128)} fusion(bf16[512,2048]{1,0:T(8,128)(2,1)} %all-gather.4.cloned.1.call-done, bf16[1,2048,1024]{2,1,0:T(8,128)(2,1)} %param.12), kind=kOutput, calls=%fused_computation.5 | convolution fusion | flops 2147483648 | bytes 8388608 | tf_op jit(solution)/shard_map/dot_general | solution.py:43
  68.2 10.0 %fusion.9 = bf16[2048,512]{0,1:T(8,128)(2,1)} fusion(bf16[1,1024,2048]{2,1,0:T(8,128)(2,1)} %param.14, f32[512,1024]{1,0:T(8,128)} %fusion.4, bf16[512,2048]{1,0:T(8,128)(2,1)S(1)} %copy-done.3, bf16[1,2048,1024]{2,1,0:T(8,128)(2,1)} %param.13), kind=kOutput, calls=%fused_computation.8 | convolution fusion | flops 4299161600 | bytes 14680064 | tf_op jit(solution)/shard_map/dot_general | solution.py:48
  78.2 31.3 %reduce-scatter.2.cloned.1.call-done = bf16[512,512]{0,1:T(8,128)(2,1)} async-done(((bf16[2048,512]{0,1:T(8,128)(2,1)}), bf16[512,512]{0,1:T(8,128)(2,1)}) %reduce-scatter.2.cloned.1.call-update) | async-done | bytes 524304 | tf_op jit(solution)/shard_map/reduce_scatter | solution.py:47
  109.6 5.5 %all-to-all-start.1 = ((bf16[512,8,64]{0,2,1:T(8,128)(2,1)}), bf16[512,8,64]{0,2,1:T(8,128)(2,1)S(1)}, u32[]{:S(2)}, u32[]{:S(2)}) async-start(bf16[512,8,64]{0,2,1:T(8,128)(2,1)} %bitcast.46), calls=%async_computation.2 | async-start | bytes 1048576 | tf_op jit(solution)/shard_map/all_to_all | solution.py:55
  115.1 0.1 copy.29
  115.2 0.1 mul.90
  115.4 0.1 copy.28
  115.5 0.1 copy.30
  115.7 13.7 %all-to-all-done.1 = bf16[512,8,64]{0,2,1:T(8,128)(2,1)S(1)} async-done(((bf16[512,8,64]{0,2,1:T(8,128)(2,1)}), bf16[512,8,64]{0,2,1:T(8,128)(2,1)S(1)}, u32[]{:S(2)}, u32[]{:S(2)}) %all-to-all-start.1) | async-done | bytes 524320 | tf_op jit(solution)/shard_map/all_to_all | solution.py:55
  129.4 1.2 gather_fusion
  130.6 0.1 gather.7
  130.7 0.8 multiply_reduce_fusion
  131.5 0.1 multiply_reduce_fusion.1
  131.6 5.9 %psum.7 = f32[128]{0:T(128)S(1)} all-reduce(f32[128]{0:T(128)S(1)} %multiply_reduce_fusion.1), channel_id=1, replica_groups=mesh['ep'=8,'tp'=4] {'tp'}, use_global_device_ids=true, to_apply=%region_9.10 | all-reduce | flops 128 | bytes 1024 | tf_op jit(solution)/shard_map/psum | solution.py:62
  137.6 0.8 fusion.20
  (21 shorter events, 0.2 us)
Async XLA Ops:
  6.5 55.1 %all-gather.4.cloned.1.call-start = ((), (), s32[]{:S(2)}) async-start(), calls=%async_computation.3 | async-start | bytes 2621440 | tf_op jit(solution)/shard_map/all_gather | solution.py:42
  39.8 69.7 %reduce-scatter.2.cloned.1.call-start = ((), (), s32[]{:S(2)}) async-start(), calls=%async_computation.4 | async-start | bytes 2621440 | tf_op jit(solution)/shard_map/reduce_scatter | solution.py:47
  61.6 6.6 %copy-start.3 = (bf16[512,2048]{1,0:T(8,128)(2,1)S(1)}, bf16[512,2048]{1,0:T(8,128)(2,1)}, u32[]{:S(2)}) copy-start(bf16[512,2048]{1,0:T(8,128)(2,1)} %all-gather.4.cloned.1.call-done) | copy-start | bytes 6291460
  78.2 36.9 %copy-start = (s32[128,2]{0,1:T(2,128)S(1)}, s32[128,2]{0,1:T(2,128)}, u32[]{:S(2)}) copy-start(s32[128,2]{0,1:T(2,128)} %param.10) | copy-start | bytes 3076
  78.2 37.3 %copy-start.1 = (f32[128,2]{0,1:T(2,128)S(1)}, f32[128,2]{0,1:T(2,128)}, u32[]{:S(2)}) copy-start(f32[128,2]{0,1:T(2,128)} %param.11) | copy-start | bytes 3076
  78.2 37.4 %copy-start.2 = (bf16[512]{0:T(512)(128)(2,1)S(1)}, bf16[512]{0:T(512)(128)(2,1)}, u32[]{:S(2)}) copy-start(bf16[512]{0:T(512)(128)(2,1)} %param.15) | copy-start | bytes 3076
  109.6 19.8 %all-to-all-start.1 = ((bf16[512,8,64]{0,2,1:T(8,128)(2,1)}), bf16[512,8,64]{0,2,1:T(8,128)(2,1)S(1)}, u32[]{:S(2)}, u32[]{:S(2)}) async-start(bf16[512,8,64]{0,2,1:T(8,128)(2,1)} %bitcast.46), calls=%async_computation.2 | async-start | bytes 1048576 | tf_op jit(solution)/shard_map/all_to_all | solution.py:55
Sparse Core Ops, SparseCore 0:
  40.0 21.5 all-gather.3
  78.4 31.1 reduce-scatter.1
